TPU v7x, 512 devices: a whole 4x4x16 slice. The times are simulated.
512 devices in a mesh: sp: 32 (over z, core), tp: 16 (over y, x).
Axes of the slice: x: 4, y: 4, z: 16, core: 2. Of those that a mesh axis runs over, the one named last changes fastest.
Arguments:
- residual_in: bfloat16 [8192, 2048], P('sp'), may hold values from -6 to 6
- queries: bfloat16 [8192, 2048], P('sp', 'tp'), may hold values from -6 to 4
- keys: bfloat16 [8192, 2048], P('sp', 'tp'), may hold values from -4 to 5.2
- values: bfloat16 [8192, 2048], P('sp', 'tp'), may hold values from -9.5 to 9.5
- out_weight: bfloat16 [2048, 2048], P('tp'), may hold values from -0.125 to 0.125
- norm_gain: float32 [2048], replicated, may hold values from 0.1 to 1.9
- expert_routes: int32 [8192, 2], P('sp'), may hold values from 0 to 31, all different within a row; in each aligned block of 256 rows (0 to 255, 256 to 511, ...) at most 32 rows name the same one
- route_scores: float32 [8192, 2], P('sp'), may hold values from -6 to 6
- gate_weight: bfloat16 [32, 2048, 4096], P('sp', None, 'tp'), may hold values from -0.125 to 0.125
- up_weight: bfloat16 [32, 2048, 4096], P('sp', None, 'tp'), may hold values from -0.125 to 0.125
- down_weight: bfloat16 [32, 4096, 2048], P('sp', 'tp'), may hold values from -0.09375 to 0.09375
Outputs:
- layer_out: bfloat16 [8192, 2048], P('sp', 'tp')
Inputs may be any that keep to these rules, and one draw needn't show every extreme that they name: `expert_routes`: each row names 2 different experts; among the 256 rows of one index of sp no expert is named more than 32 times, and in every draw some such block names some expert exactly 32 times.
All inputs are finite; a program needn't handle non-finite values.
Results may differ from a plain program's by a relative error of at most 0.015.
Values may be sent and summed in bfloat16 or wider, within the bound.
No kernel may reach another device: no remote copies, remote signals or barrier semaphores. Data moves between devices by JAX's collectives and lax.ppermute only.
A program may use at most 64 MiB of HBM per device.

v0:
```python
import jax
import jax.numpy as jnp
from jax import lax
from jax.sharding import PartitionSpec as P

HD = 64


epsilon = 1e-06


def in_one_piece(arrays, axis, dim, along):
    both = jnp.concatenate(arrays, axis=along)
    filled, at, outs = (lax.all_gather(both, axis, axis=dim, tiled=True), 0, [])
    for a in arrays:
        outs.append(lax.slice_in_dim(filled, at, at + a.shape[along], axis=along))
        at += a.shape[along]
    return tuple(outs)


def padded_to(lines, peers):
    spare = -len(lines) % peers
    return jnp.pad(lines, [(0, spare)] + [(0, 0)] * (lines.ndim - 1))


def copy_for_each(shard, axis):
    copies = jnp.broadcast_to(shard, (lax.axis_size(axis), *shard.shape))
    return lax.all_to_all(copies, axis, split_axis=0, concat_axis=0, tiled=True)


def joined_along(pieces, dim):
    pieces = jnp.moveaxis(pieces, 0, dim)
    dims = pieces.shape
    return pieces.reshape(*dims[:dim], dims[dim] * dims[dim + 1], *dims[dim + 2 :])


def gathered_copies(shard, axis, dim):
    pieces = copy_for_each(shard, axis)
    return joined_along(pieces, dim)


def cut_along(shard, dim, peers):
    dims = shard.shape
    pieces = shard.reshape(*dims[:dim], peers, dims[dim] // peers, *dims[dim + 1 :])
    return jnp.moveaxis(pieces, dim, 0)


def summed_on_arrival(shard, axis, dim):
    peers = lax.axis_size(axis)
    pieces = lax.all_to_all(cut_along(shard, dim, peers), axis, 0, 0, tiled=True)
    return jnp.sum(pieces.astype(jnp.float32), axis=0)


def nested_sum(shard, axes):
    lines = shard.reshape(-1, shard.shape[-1])
    padded = padded_to(lines, lax.axis_size(axes))
    whole = gathered_copies(summed_on_arrival(padded, axes, 0).astype(jnp.bfloat16), axes, 0)
    return lax.slice_in_dim(whole, 0, len(lines)).reshape(shard.shape).astype(jnp.float32)


def attend(queries, query_start, keys_all, values_all):
    row_count = queries.shape[0]
    total_len = keys_all.shape[0]
    head_count = queries.shape[1] // HD
    span = min(512, total_len)
    scale = HD ** (-0.5)
    query_heads = queries.reshape(row_count, head_count, HD)
    query_pos = query_start + lax.iota(jnp.int32, row_count)
    block_count = (query_start + row_count - 1 + span - 1) // span

    def one_block(step_index, state_pair):
        accumulated, kept_log = state_pair
        key_start = (block_count - 1 - step_index) * span
        key_block = lax.dynamic_slice_in_dim(keys_all, key_start, span, 0).reshape(
            span, head_count, HD
        )
        value_block = lax.dynamic_slice_in_dim(values_all, key_start, span, 0).reshape(
            span, head_count, HD
        )
        scores = (
            jnp.einsum("qhc,khc->hqk", query_heads, key_block, preferred_element_type=jnp.float32)
            * scale
        )
        key_pos = key_start + lax.iota(jnp.int32, span)
        causal = key_pos[None, :] < query_pos[:, None]
        log_keep = jnp.where(causal, jax.nn.log_sigmoid(-scores), 0.0)
        between = lax.cumsum(log_keep, axis=2, reverse=True) - log_keep + kept_log[:, :, None]
        weights = jnp.where(causal, jnp.exp(jax.nn.log_sigmoid(scores) + between), 0.0).astype(
            jnp.bfloat16
        )
        accumulated = accumulated + jnp.einsum(
            "hqk,khc->qhc", weights, value_block, preferred_element_type=jnp.float32
        )
        return (accumulated, kept_log + jnp.sum(log_keep, axis=2))

    start_pair = (
        jnp.zeros((row_count, head_count, HD), jnp.float32),
        jnp.zeros((head_count, row_count), jnp.float32),
    )
    accumulated, kept_log = lax.fori_loop(0, block_count, one_block, start_pair)
    return accumulated.reshape(row_count, head_count * HD).astype(jnp.bfloat16)


def route_targets(routes, experts, capacity):
    flat_routes = routes.reshape(-1)
    onehot = (flat_routes[:, None] == lax.iota(jnp.int32, experts)[None, :]).astype(jnp.int32)
    before = jnp.cumsum(onehot, axis=0) - onehot
    return flat_routes * capacity + jnp.sum(before * onehot, axis=1)


def shards(
    residual_in,
    queries,
    keys,
    values,
    out_weight,
    norm_gain,
    expert_routes,
    route_scores,
    gate_weight,
    up_weight,
    down_weight,
):
    row_count = residual_in.shape[0]
    width = residual_in.shape[1]
    row_start = lax.axis_index("sp") * row_count
    keys_all, values_all = in_one_piece((keys, values), "sp", 0, 1)
    mixed_heads = attend(queries, row_start, keys_all, values_all)
    partial_value = jnp.dot(mixed_heads, out_weight, preferred_element_type=jnp.float32).astype(
        jnp.bfloat16
    )
    attended = nested_sum(partial_value, "tp").astype(jnp.bfloat16)
    stream = (residual_in.astype(jnp.float32) + attended.astype(jnp.float32)).astype(jnp.bfloat16)
    stream_wide = stream.astype(jnp.float32)
    normed = (
        stream_wide
        * lax.rsqrt(jnp.mean(stream_wide * stream_wide, axis=1, keepdims=True) + epsilon)
        * norm_gain
    ).astype(jnp.bfloat16)
    experts = lax.axis_size("sp")
    capacity = 4 * row_count // experts
    top_count = expert_routes.shape[1]
    targets = route_targets(expert_routes, experts, capacity)
    owners = lax.iota(jnp.int32, row_count * top_count) // top_count
    slot_owner = jnp.full((experts * capacity,), row_count, jnp.int32).at[targets].set(owners)
    padded = jnp.concatenate([normed, jnp.zeros((1, width), jnp.bfloat16)], axis=0)
    outgoing = padded[slot_owner].reshape(experts, capacity, width)
    col_count = width // lax.axis_size("tp")
    column_start = lax.axis_index("tp") * col_count
    own_part = lax.dynamic_slice_in_dim(outgoing, column_start, col_count, 2)
    arrived = lax.all_to_all(own_part, "sp", split_axis=0, concat_axis=0, tiled=True)
    arrived = gathered_copies(arrived, "tp", 2)
    slot_rows = arrived.reshape(-1, width)
    gate_act = jnp.dot(slot_rows, gate_weight[0], preferred_element_type=jnp.float32)
    up_act = jnp.dot(slot_rows, up_weight[0], preferred_element_type=jnp.float32)
    hidden = (jax.nn.silu(gate_act) * up_act).astype(jnp.bfloat16)
    expert_part = (
        jnp.dot(hidden, down_weight[0], preferred_element_type=jnp.float32)
        .astype(jnp.bfloat16)
        .reshape(arrived.shape)
    )
    summed = summed_on_arrival(expert_part, "tp", 2).astype(jnp.bfloat16)
    returned = lax.all_to_all(summed, "sp", split_axis=0, concat_axis=0, tiled=True)
    results = returned.reshape(experts * capacity, col_count)
    picked = results[targets].astype(jnp.float32).reshape(row_count, top_count, col_count)
    shares = jax.nn.sigmoid(route_scores - route_scores[:, ::-1])
    combined = jnp.sum(picked * shares[:, :, None], axis=1)
    own_columns = lax.dynamic_slice_in_dim(stream_wide, column_start, col_count, 1)
    return (own_columns + combined).astype(jnp.bfloat16)


def solution(mesh):
    in_specs = (
        P("sp", None),
        P("sp", "tp"),
        P("sp", "tp"),
        P("sp", "tp"),
        P("tp", None),
        P(),
        P("sp", None),
        P("sp", None),
        P("sp", None, "tp"),
        P("sp", None, "tp"),
        P("sp", "tp", None),
    )
    out_specs = P("sp", "tp")
    return jax.shard_map(shards, mesh=mesh, in_specs=in_specs, out_specs=out_specs, check_vma=False)
```

profile of v0, /device:TPU:1, one launch (start us, length us, event | category | flops | bytes accessed | tf_op | source)
XLA Modules:
  0.0 564.1 jit_solution(7993542427188019450)
XLA Ops:
  6.5 1.0 copy.33
  10.2 85.7 %all-gather.2.cloned.1.call-done = bf16[8192,256]{0,1:T(8,128)(2,1)} async-done(((bf16[256,256]{0,1:T(8,128)(2,1)}), bf16[8192,256]{0,1:T(8,128)(2,1)}) %all-gather.2.cloned.1.call-update) | async-done | bytes 4194320 | tf_op jit(solution)/shard_map/all_gather | solution.py:14
  95.8 4.6 fusion.49
  101.1 13.0 %while.15 = (s32[]{:T(128)}, f32[256,2,64]{0,2,1:T(8,128)S(1)}, f32[2,256]{1,0:T(2,128)}, s32[]{:T(128)}, s32[]{:T(128)}, /*index=5*/bf16[8192,128]{0,1:T(8,128)...) while((s32[]{:T(128)}, f32[256,2,64]{0,2,1:T(8,128)S(1)}, ...), condition=%wide.region_4.5_spmd.clone, body=%wide.region_0.4_spmd.clone.sunk | while | flops 108962056 | bytes 13650211 | solution.py:100
  102.3 1.6 fusion.70
  103.8 4.8 fusion.71
  110.4 2.2 fusion.72
  112.8 1.3 add.244
  114.1 2.6 convolution_convert_fusion
  116.7 6.5 %all-to-all-start = ((bf16[16,16,2048]{2,1,0:T(8,128)(2,1)}), bf16[16,16,2048]{2,1,0:T(8,128)(2,1)S(1)}, u32[]{:S(2)}, u32[]{:S(2)}) async-start(bf16[16,16,2048]{2,1,0:T(8,128)(2,1)} %bitcast.119), calls=%async_computation | async-start | bytes 2097152 | tf_op jit(solution)/shard_map/all_to_all | solution.py:50
  124.3 1.2 reduce-window.24
  125.5 14.1 %all-to-all-done = bf16[16,16,2048]{2,1,0:T(8,128)(2,1)S(1)} async-done(((bf16[16,16,2048]{2,1,0:T(8,128)(2,1)}), bf16[16,16,2048]{2,1,0:T(8,128)(2,1)S(1)}, u32[]{:S(2)}, u32[]{:S(2)}) %all-to-all-start) | async-done | bytes 1048608 | tf_op jit(solution)/shard_map/all_to_all | solution.py:50
  139.8 1.1 broadcast_in_dim.40
  140.9 4.5 all-to-all-start.1
  146.1 2.4 scatter_custom_fusion
  148.6 12.7 %all-to-all-done.1 = bf16[16,16,2048]{2,1,0:T(8,128)(2,1)S(1)} async-done(((bf16[16,16,2048]{2,1,0:T(8,128)(2,1)}), bf16[16,16,2048]{2,1,0:T(8,128)(2,1)S(1)}, u32[]{:S(2)}, u32[]{:S(2)}) %all-to-all-start.1) | async-done | bytes 1048608 | tf_op jit(solution)/shard_map/all_to_all | solution.py:28
  161.3 1.7 fusion.28
  163.7 6.0 %gather_fusion = bf16[1024,2048]{1,0:T(8,128)(2,1)} fusion(bf16[257,2048]{1,0:T(8,128)(2,1)S(1)} %concatenate.7, s32[1024]{0:T(1024)S(1)} %fusion.42), kind=kCustom, calls=%fused_computation | custom fusion | bytes 8392704 | tf_op jit(solution)/shard_map/gather | solution.py:147
  170.7 222.3 %all_to_all.30 = bf16[32,32,128]{2,1,0:T(8,128)(2,1)S(1)} all-to-all(bf16[32,32,128]{2,1,0:T(8,128)(2,1)S(1)} %constant_dynamic-slice_fusion.2), channel_id=1, replica_groups=mesh['sp'=32,'tp'=16] {'sp'}, dimensions={0} | all-to-all | bytes 524288 | tf_op jit(solution)/shard_map/all_to_all | solution.py:151
  393.8 52.7 %all_to_all.31 = bf16[16,32,32,128]{3,2,1,0:T(8,128)(2,1)S(1)} all-to-all(bf16[16,32,32,128]{3,2,1,0:T(8,128)(2,1)S(1)} %broadcast_in_dim.43), channel_id=1, replica_groups=mesh['sp'=32,'tp'=16] {'tp'}, dimensions={0} | all-to-all | bytes 8388608 | tf_op jit(solution)/shard_map/all_to_all | solution.py:28
  446.5 4.9 copy.40
  451.4 1.9 copy-done.2
  453.3 1.3 fusion.17
  454.6 8.5 %convert_bitcast_fusion = bf16[128,8,16,128]{3,1,2,0:T(8,128)(2,1)} fusion(bf16[1,256,2048]{2,1,0:T(8,128)(2,1)S(1)} %copy-done, bf16[128,8,16,128]{3,2,1,0:T(8,128)(2,1)} %bitcast.118, bf16[1,2048,256]{2,1,0:T(8,128)(2,1)S(1)} %copy-done.10, f32[1024,256]{1,0:T(8,128)S(1)} %fusion.17), kind=kOutput, calls=%fused_computation.34 | convolution fusion | flops 2151153664 | bytes 11534336 | tf_op jit(solution)/shard_map/dot_general | solution.py:158
  463.1 3.6 copy.46
  466.7 1.3 copy.65
  468.0 53.2 %all_to_all.32 = bf16[16,32,32,128]{3,2,1,0:T(8,128)(2,1)} all-to-all(bf16[16,32,32,128]{3,2,1,0:T(8,128)(2,1)S(1)} %bitcast.113), channel_id=1, replica_groups=mesh['sp'=32,'tp'=16] {'tp'}, dimensions={0} | all-to-all | bytes 8388608 | tf_op jit(solution)/shard_map/all_to_all | solution.py:50
  521.1 3.5 reduce_sum.68
  524.7 7.0 %all-to-all-start.5 = ((bf16[32,32,128]{2,1,0:T(8,128)(2,1)}), bf16[32,32,128]{2,1,0:T(8,128)(2,1)S(1)}, u32[]{:S(2)}, u32[]{:S(2)}) async-start(bf16[32,32,128]{2,1,0:T(8,128)(2,1)} %reduce_sum.68), calls=%async_computation.5 | async-start | bytes 524288 | tf_op jit(solution)/shard_map/all_to_all | solution.py:163
  531.9 22.0 %all-to-all-done.5 = bf16[32,32,128]{2,1,0:T(8,128)(2,1)S(1)} async-done(((bf16[32,32,128]{2,1,0:T(8,128)(2,1)}), bf16[32,32,128]{2,1,0:T(8,128)(2,1)S(1)}, u32[]{:S(2)}, u32[]{:S(2)}) %all-to-all-start.5) | async-done | bytes 262176 | tf_op jit(solution)/shard_map/all_to_all | solution.py:163
  553.9 1.3 gather_fusion.1
  555.7 1.6 add_convert_fusion
  (64 shorter events, 11.3 us)
Async XLA Ops:
  6.5 448.0 %copy-start = (bf16[1,256,2048]{2,1,0:T(8,128)(2,1)S(1)}, bf16[1,256,2048]{2,1,0:T(8,128)(2,1)}, u32[]{:S(2)}) copy-start(bf16[1,256,2048]{2,1,0:T(8,128)(2,1)} %param.23) | copy-start | bytes 3145732
  6.5 89.3 %all-gather.2.cloned.1.call-start = ((), (), s32[]{:S(2)}) async-start(), calls=%async_computation.6 | async-start | bytes 4325376 | tf_op jit(solution)/shard_map/all_gather | solution.py:14
  101.1 2.8 copy-start.3
  109.9 2.8 copy-start.5
  110.2 3.9 copy-start.4
  114.1 31.6 %copy-start.7 = (s32[256,2]{0,1:T(2,128)S(1)}, s32[256,2]{0,1:T(2,128)}, u32[]{:S(2)}) copy-start(s32[256,2]{0,1:T(2,128)} %param.19) | copy-start | bytes 6148
  114.1 47.2 %copy-start.1 = (bf16[256,2048]{1,0:T(8,128)(2,1)S(1)}, bf16[256,2048]{1,0:T(8,128)(2,1)}, u32[]{:S(2)}) copy-start(bf16[256,2048]{1,0:T(8,128)(2,1)} %param.13) | copy-start | bytes 3145732
  116.7 23.0 %all-to-all-start = ((bf16[16,16,2048]{2,1,0:T(8,128)(2,1)}), bf16[16,16,2048]{2,1,0:T(8,128)(2,1)S(1)}, u32[]{:S(2)}, u32[]{:S(2)}) async-start(bf16[16,16,2048]{2,1,0:T(8,128)(2,1)} %bitcast.119), calls=%async_computation | async-start | bytes 2097152 | tf_op jit(solution)/shard_map/all_to_all | solution.py:50
  139.8 23.3 %copy-start.6 = (f32[2048]{0:T(1024)S(1)}, f32[2048]{0:T(1024)}, u32[]{:S(2)}) copy-start(f32[2048]{0:T(1024)} %param.18) | copy-start | bytes 24580
  140.9 20.4 %all-to-all-start.1 = ((bf16[16,16,2048]{2,1,0:T(8,128)(2,1)}), bf16[16,16,2048]{2,1,0:T(8,128)(2,1)S(1)}, u32[]{:S(2)}, u32[]{:S(2)}) async-start(bf16[16,16,2048]{2,1,0:T(8,128)(2,1)} %broadcast_in_dim.40), calls=%async_computation.1 | async-start | bytes 2097152 | tf_op jit(solution)/shard_map/all_to_all | solution.py:28
  446.5 6.8 %copy-start.9 = (bf16[1,2048,256]{2,1,0:T(8,128)(2,1)S(1)}, bf16[1,2048,256]{2,1,0:T(8,128)(2,1)}, u32[]{:S(2)}) copy-start(bf16[1,2048,256]{2,1,0:T(8,128)(2,1)} %param.21) | copy-start | bytes 3145732
  451.4 1.9 copy-start.2
  453.3 1.3 copy-start.10
  521.1 10.5 %copy-start.8 = (f32[256,2]{0,1:T(2,128)S(1)}, f32[256,2]{0,1:T(2,128)}, u32[]{:S(2)}) copy-start(f32[256,2]{0,1:T(2,128)} %param.20) | copy-start | bytes 6148
  524.7 29.2 %all-to-all-start.5 = ((bf16[32,32,128]{2,1,0:T(8,128)(2,1)}), bf16[32,32,128]{2,1,0:T(8,128)(2,1)S(1)}, u32[]{:S(2)}, u32[]{:S(2)}) async-start(bf16[32,32,128]{2,1,0:T(8,128)(2,1)} %reduce_sum.68), calls=%async_computation.5 | async-start | bytes 524288 | tf_op jit(solution)/shard_map/all_to_all | solution.py:163
Sparse Core Ops, SparseCore 0:
  9.4 86.4 all-gather.1
where the time goes:
time: 567 us; the launch traced here: 564 us
  blocking collectives  328 us (58%)
  waiting for transfers between devices  135 us (24%)
  local copies, waits for them, and re-layouts  36.3 us (6%)
  other arithmetic  19.3 us (3%)
  starting transfers between devices  18 us (3%)
  matrix products  14.1 us (2%)
  between operations  13.7 us (2%)
    all_to_all x1, blocking collectives, shards(): lax.all_to_all(own_part, 'sp', split_axis=0, concat_axis=0, tiled=True)  222 us
    all_gather x1, waiting for transfers between devices, in_one_piece(): filled, at, outs = (lax.all_gather(both, axis, axis=dim, tiled=True), 0, [])  85.7 us
    all_to_all x1, blocking collectives, summed_on_arrival(): lax.all_to_all(cut_along(shard, dim, peers), axis, 0, 0, tiled=True)  53.2 us
    all_to_all x1, blocking collectives, copy_for_each(): return lax.all_to_all(copies, axis, split_axis=0, concat_axis=0, tiled=True)  52.7 us
    all_to_all x1, waiting for transfers between devices, shards(): lax.all_to_all(summed, 'sp', split_axis=0, concat_axis=0, tiled=True)  22 us
    all_to_all x1, waiting for transfers between devices, summed_on_arrival(): lax.all_to_all(cut_along(shard, dim, peers), axis, 0, 0, tiled=True)  14.1 us
    all_to_all x1, waiting for transfers between devices, copy_for_each(): return lax.all_to_all(copies, axis, split_axis=0, concat_axis=0, tiled=True)  12.7 us
  transfers between devices with their start and end apart: 4, of which 4 were waited for; matrix products, arithmetic and copies ran while one was open for 1% of the time, Pallas kernels for 0%

commit v1 on v0

v1 whole, which is shorter than its diff:
```python
import functools

import jax
import jax.numpy as jnp
from jax import lax
from jax.experimental import pallas as pl
from jax.experimental.pallas import tpu as pltpu
from jax.sharding import Mesh, PartitionSpec as P

HD = 64
LANES = 128
ROWS = 256
EPSILON = 1e-06
BF = jnp.bfloat16
F32 = jnp.float32
VM = pl.BlockSpec(memory_space=pltpu.VMEM)
SM = pl.BlockSpec(memory_space=pltpu.SMEM)


def call(body, out_shape, specs, **more):
    return pl.pallas_call(body, out_shape=out_shape, in_specs=specs, **more)


def shaped(dims, dtype=BF):
    return jax.ShapeDtypeStruct(dims, dtype)


def lane_ids(dims):
    return lax.broadcasted_iota(jnp.int32, dims, len(dims) - 1)


def dot(a, b):
    return jnp.dot(a, b, preferred_element_type=F32)


def pack_body(q_ref, k_ref, v_ref, out_ref):
    q, k, v = (r[...].astype(F32) for r in (q_ref, k_ref, v_ref))
    low = lane_ids(q.shape) < HD
    q = q * (HD**-0.5)
    q_turned, k_turned, v_turned = (pltpu.roll(a, HD, 1) for a in (q, k, v))
    out_ref[0, 0] = jnp.where(low, k, v_turned).astype(BF)
    out_ref[1, 0] = jnp.where(low, k_turned, v).astype(BF)
    out_ref[0, 1] = jnp.where(low, q, 0.0).astype(BF)
    out_ref[1, 1] = jnp.where(low, q_turned, 0.0).astype(BF)


def tile(q, kv, later, mask):
    z = lax.dot_general(q, kv, (((1,), (1,)), ((), ())), preferred_element_type=F32)
    if mask is not None:
        z = jnp.where(mask, z, -1e30)
    kept = jnp.maximum(z, jnp.log(1.0 + jnp.exp(jnp.minimum(z, 80.0))))
    after = dot(kept.astype(BF), later)
    weights = jnp.exp((z - kept) - after).astype(BF)
    return dot(weights, kv), after[:, :1] + kept[:, :1]


def attend_body(z_ref, q_ref, kv_ref, later_ref, out_ref, *, step):
    z = z_ref[0]
    later = later_ref[...]
    causal = lane_ids((ROWS, ROWS)) < lax.broadcasted_iota(jnp.int32, (ROWS, ROWS), 0)
    parts = 2 * ROWS // step
    qs = [q_ref[i * step : (i + 1) * step] for i in range(parts)]
    base = z * (2 * ROWS)
    kv0 = kv_ref[pl.ds(pl.multiple_of(base, ROWS), ROWS)]
    kv1 = kv_ref[pl.ds(pl.multiple_of(base + ROWS, ROWS), ROWS)]
    state = []
    for i in range(parts):
        half, at = divmod(i * step, ROWS)
        mask = causal[at : at + step]
        if half == 0:
            out, total = tile(qs[i], kv0, later, mask)
        else:
            out, total = tile(qs[i], kv1, later, mask)
            more, further = tile(qs[i], kv0, later, None)
            out, total = out + jnp.exp(-total) * more, total + further
        state.append((out, total))

    def one(j, state):
        at = pl.multiple_of((2 * z - 1 - j) * ROWS, ROWS)
        kv = kv_ref[pl.ds(at, ROWS)]
        new = []
        for q, (out, total) in zip(qs, state):
            more, further = tile(q, kv, later, None)
            new.append((out + jnp.exp(-total) * more, total + further))
        return tuple(new)

    state = lax.fori_loop(0, 2 * z, one, tuple(state))
    outs = jnp.concatenate([s[0] for s in state], axis=0)
    low = lane_ids((ROWS // 2, LANES)) < HD
    for block in range(2):
        top = outs[block * ROWS : block * ROWS + ROWS // 2]
        bottom = outs[block * ROWS + ROWS // 2 : (block + 1) * ROWS]
        both = jnp.where(low, pltpu.roll(top, HD, 1), bottom).astype(BF)
        for peer in range(out_ref.shape[1]):
            out_ref[block, peer] = both


def route_body(col_ref, row_ref, col_out, row_out, *, experts, cap):
    below = (lane_ids((ROWS, ROWS)) < lax.broadcasted_iota(jnp.int32, (ROWS, ROWS), 0)).astype(F32).astype(BF)
    above = (lane_ids((ROWS, ROWS)) > lax.broadcasted_iota(jnp.int32, (ROWS, ROWS), 0)).astype(F32).astype(BF)
    ids = lane_ids((ROWS, LANES))
    hot = [(ids == col_ref[:, k : k + 1]).astype(F32) for k in range(2)]
    before = dot(below, (hot[0] + hot[1]).astype(BF))
    for k in range(2):
        place = jnp.sum(before * hot[k], axis=1, keepdims=True).astype(jnp.int32)
        col_out[:, k : k + 1] = col_ref[:, k : k + 1] * cap + place
    ids = lax.broadcasted_iota(jnp.int32, (experts, ROWS), 0)
    hot = [(ids == row_ref[k : k + 1]).astype(F32) for k in range(2)]
    before = dot((hot[0] + hot[1]).astype(BF), above)
    for k in range(2):
        place = jnp.sum(before * hot[k], axis=0, keepdims=True).astype(jnp.int32)
        row_out[k : k + 1] = row_ref[k : k + 1] * cap + place


def project_body(mixed_ref, ow_ref, res_ref, row_ref, stream_ref, out_ref):
    tp = ow_ref.shape[0]
    nothing = jnp.zeros((HD, LANES), BF)
    total = jnp.zeros((ROWS // 2, 2 * LANES), F32)
    for t in range(tp):
        pieces, weights = [], []
        for c in range(2):
            w = ow_ref[t, c * HD : (c + 1) * HD]
            pieces.append(mixed_ref[c * tp + t])
            weights.append(jnp.concatenate([w, nothing], axis=1))
            weights.append(jnp.concatenate([nothing, w], axis=1))
        total = total + dot(jnp.concatenate(pieces, axis=1), jnp.concatenate(weights, axis=0))
    attended = jnp.concatenate([total[:, :LANES], total[:, LANES:]], axis=0).astype(BF)
    stream = (res_ref[...].astype(F32) + attended.astype(F32)).astype(BF)
    stream_ref[...] = stream
    slots = lax.broadcasted_iota(jnp.int32, (out_ref.shape[0], ROWS), 0)
    owned = (slots == row_ref[0:1]) | (slots == row_ref[1:2])
    out_ref[...] = dot(owned.astype(F32).astype(BF), stream).astype(BF)


def expert_body(x_ref, gain_ref, gate_ref, up_ref, down_ref, out_ref):
    tp, rows = x_ref.shape[0], x_ref.shape[1]
    wide = [x_ref[i].astype(F32) for i in range(tp)]
    squares = wide[0] * wide[0]
    for w in wide[1:]:
        squares = squares + w * w
    mean = jnp.sum(squares, axis=1, keepdims=True) * (1.0 / (tp * LANES))
    factor = lax.rsqrt(mean + EPSILON)
    normed = [(w * factor * gain_ref[i : i + 1]).astype(BF) for i, w in enumerate(wide)]
    normed = jnp.concatenate(normed, axis=1)
    gate = dot(normed, gate_ref[...])
    up = dot(normed, up_ref[...])
    hidden = (gate / (1.0 + jnp.exp(-gate)) * up).astype(BF)
    for i in range(tp):
        out_ref[i] = dot(hidden, down_ref[:, i * LANES : (i + 1) * LANES]).astype(BF)


def sum_body(x_ref, out_ref):
    total = x_ref[0].astype(F32)
    for i in range(1, x_ref.shape[0]):
        total = total + x_ref[i].astype(F32)
    out_ref[...] = total.astype(BF)


def combine_body(x_ref, col_ref, score_ref, stream_ref, out_ref):
    x = x_ref[...]
    slots = lane_ids((ROWS, x.shape[0]))
    gap = score_ref[:, 0:1] - score_ref[:, 1:2]
    total = 0.0
    for k in range(2):
        owned = (slots == col_ref[:, k : k + 1]).astype(F32).astype(BF)
        share = 1.0 / (1.0 + jnp.exp(-gap if k == 0 else gap))
        total = total + share * dot(owned, x)
    out_ref[...] = (stream_ref[...].astype(F32) + total).astype(BF)


def shards(residual_in, queries, keys, values, out_weight, norm_gain, expert_routes, route_scores, gate_weight, up_weight, down_weight):
    zs, tp = lax.axis_size("z"), lax.axis_size("tp")
    experts = 2 * zs
    cap = 4 * ROWS // experts
    slots = experts * cap
    width = residual_in.shape[1]
    here = lax.axis_index("tp")

    packed = call(pack_body, shaped((2, 2, ROWS, LANES)), [VM] * 3)(queries, keys, values)
    packed = lax.all_to_all(packed, "core", 0, 0, tiled=True)
    own_kv = packed[:, 0].reshape(2 * ROWS, LANES)
    own_q = packed[:, 1].reshape(2 * ROWS, LANES)
    kv = lax.all_gather(own_kv, "z", axis=0, tiled=True)

    own_ow = jnp.moveaxis(out_weight.reshape(LANES, tp, LANES), 1, 0)
    own_ow = lax.all_to_all(own_ow, "tp", 0, 0, tiled=True)
    to_col, to_row = call(
        functools.partial(route_body, experts=experts, cap=cap),
        [shaped((ROWS, 2), jnp.int32), shaped((2, ROWS), jnp.int32)],
        [VM] * 2,
        out_specs=[VM] * 2,
    )(expert_routes, expert_routes.T)
    own_res = lax.dynamic_slice_in_dim(residual_in, here * LANES, LANES, 1)

    later = (lax.iota(jnp.int32, ROWS)[:, None] > lax.iota(jnp.int32, ROWS)[None, :]).astype(BF)
    place = lax.axis_index("z").reshape(1).astype(jnp.int32)
    mixed = call(
        functools.partial(attend_body, step=128),
        shaped((2, tp, ROWS // 2, LANES)),
        [SM, VM, VM, VM],
    )(place, own_q, kv, later)
    mixed = lax.all_to_all(mixed.reshape(2 * tp, ROWS // 2, LANES), ("core", "tp"), 0, 0, tiled=True)

    stream, outgoing = call(
        project_body,
        [shaped((ROWS, LANES)), shaped((slots, LANES))],
        [VM] * 4,
        out_specs=[VM] * 2,
    )(mixed, own_ow, own_res, to_row)
    arrived = lax.all_to_all(outgoing.reshape(experts, cap, LANES), ("z", "core"), 0, 0, tiled=True)
    copies = jnp.broadcast_to(arrived.reshape(1, slots, LANES), (tp, slots, LANES))
    arrived = lax.all_to_all(copies, "tp", 0, 0, tiled=True)

    chunk = 256
    whole = lambda i: (0, 0)
    parts = pl.pallas_call(
        expert_body,
        out_shape=shaped((tp, slots, LANES)),
        grid=(slots // chunk,),
        in_specs=[
            pl.BlockSpec((tp, chunk, LANES), lambda i: (0, i, 0)),
            pl.BlockSpec((tp, LANES), whole),
            pl.BlockSpec(gate_weight.shape[1:], whole),
            pl.BlockSpec(up_weight.shape[1:], whole),
            pl.BlockSpec(down_weight.shape[1:], whole),
        ],
        out_specs=pl.BlockSpec((tp, chunk, LANES), lambda i: (0, i, 0)),
    )(arrived, norm_gain.reshape(tp, LANES), gate_weight[0], up_weight[0], down_weight[0])
    parts = lax.all_to_all(parts, "tp", 0, 0, tiled=True)
    summed = pl.pallas_call(
        sum_body,
        out_shape=shaped((slots, LANES)),
        grid=(slots // chunk,),
        in_specs=[pl.BlockSpec((tp, chunk, LANES), lambda i: (0, i, 0))],
        out_specs=pl.BlockSpec((chunk, LANES), lambda i: (i, 0)),
    )(parts)
    returned = lax.all_to_all(summed.reshape(experts, cap, LANES), ("z", "core"), 0, 0, tiled=True)
    return call(combine_body, shaped((ROWS, LANES)), [VM] * 4)(
        returned.reshape(slots, LANES), to_col, route_scores, stream
    )


def solution(mesh):
    sp, tp = mesh.devices.shape
    fine = Mesh(mesh.devices.reshape(sp // 2, 2, tp), ("z", "core", "tp"))
    rows = ("z", "core")
    in_specs = (
        P(rows, None),
        P(rows, "tp"),
        P(rows, "tp"),
        P(rows, "tp"),
        P("tp", None),
        P(),
        P(rows, None),
        P(rows, None),
        P(rows, None, "tp"),
        P(rows, None, "tp"),
        P(rows, "tp", None),
    )
    return jax.shard_map(shards, mesh=fine, in_specs=in_specs, out_specs=P(rows, "tp"), check_vma=False)
```

time: 567 us -> 344 us (0.61)
  blocking collectives: 328 us -> 177 us
  waiting for transfers between devices: 135 us -> 90.3 us
  local copies, waits for them, and re-layouts: 36.3 us -> 7.78 us
  Pallas kernels: 0 us -> 26.5 us
  other arithmetic: 19.3 us -> 0.66 us
  matrix products: 14.1 us -> 0 us
  starting transfers between devices: 18 us -> 27.5 us
    all_to_all x3 -> x4, blocking collectives: 328 us -> 177 us  [the longest x1 57.7 us: shards(): lax.all_to_all(outgoing.reshape(experts, cap, LANES), ('z', 'core'), 0, 0...]
    all_gather x1, waiting for transfers between devices: 85.7 us -> 55.7 us  [shards(): kv = lax.all_gather(own_kv, 'z', axis=0, tiled=True)]
    pallas_call x0 -> x7, Pallas kernels: none -> 26.5 us  [the longest x1 9.5 us: shards(): pl.pallas_call(expert_body, out_shape=shaped((tp, slots, LANES)), grid=(s...]
    all_to_all x3, waiting for transfers between devices: 48.8 us -> 34.5 us  [the longest x1 21.5 us: shards(): lax.all_to_all(summed.reshape(experts, cap, LANES), ('z', 'core'), 0, 0,...]
    dot_general x5 -> x0, matrix products: 14.1 us -> none  [the longest x1 8.5 us: shards(): jnp.dot(hidden, down_weight[0], preferred_element_type=jnp.float32)]
    all_to_all x3, starting transfers between devices: 18 us -> 27.5 us  [the longest x1 16.8 us: shards(): lax.all_to_all(mixed.reshape(2 * tp, ROWS // 2, LANES), ('core', 'tp'), 0...]
    gather x2 -> x0, local copies, waits for them, and re-layouts: 7.35 us -> none  [the longest x1 6.02 us: shards(): outgoing = padded[slot_owner].reshape(experts, capacity, width)]
    another operation x5 -> x0, other arithmetic: 6.9 us -> none
  transfers between devices with their start and end apart: 4 -> 4, of which waited for: 4 -> 3; matrix products, arithmetic and copies ran while one was open for 1% -> 2% of each run, Pallas kernels for 0% -> 2%
where the time goes in v1:
time: 344 us; the launch traced here: 343 us
  blocking collectives  177 us (51%)
  waiting for transfers between devices  90.3 us (26%)
  starting transfers between devices  27.5 us (8%)
  Pallas kernels  26.5 us (8%)
  between operations  13.5 us (4%)
  local copies, waits for them, and re-layouts  7.78 us (2%)
    all_to_all x1, blocking collectives, shards(): lax.all_to_all(outgoing.reshape(experts, cap, LANES), ('z', 'core'), 0, 0...  57.7 us
    all_gather x1, waiting for transfers between devices, shards(): kv = lax.all_gather(own_kv, 'z', axis=0, tiled=True)  55.7 us
    all_to_all x1, blocking collectives, shards(): parts = lax.all_to_all(parts, 'tp', 0, 0, tiled=True)  54.3 us
    all_to_all x1, blocking collectives, shards(): arrived = lax.all_to_all(copies, 'tp', 0, 0, tiled=True)  53.4 us
    all_to_all x1, waiting for transfers between devices, shards(): lax.all_to_all(summed.reshape(experts, cap, LANES), ('z', 'core'), 0, 0,...  21.5 us
    all_to_all x1, starting transfers between devices, shards(): lax.all_to_all(mixed.reshape(2 * tp, ROWS // 2, LANES), ('core', 'tp'), 0...  16.8 us
    all_to_all x1, waiting for transfers between devices, shards(): lax.all_to_all(mixed.reshape(2 * tp, ROWS // 2, LANES), ('core', 'tp'), 0...  13.1 us
    all_to_all x1, blocking collectives, shards(): packed = lax.all_to_all(packed, 'core', 0, 0, tiled=True)  11.5 us
  transfers between devices with their start and end apart: 4, of which 3 were waited for; matrix products, arithmetic and copies ran while one was open for 2% of the time, Pallas kernels for 2%

profile of v1, /device:TPU:1, one launch (start us, length us, event | category | flops | bytes accessed | tf_op | source)
XLA Modules:
  0.0 343.1 jit_solution(9097542005233612543)
XLA Ops:
  6.5 0.0 copy-start
  6.5 1.8 shard_map.109
  8.3 11.5 %all_to_all.35 = bf16[2,2,256,128]{3,2,1,0:T(8,128)(2,1)S(1)} all-to-all(bf16[2,2,256,128]{3,2,1,0:T(8,128)(2,1)} %shard_map.109), channel_id=1, replica_groups=mesh['z'=16,'core'=2,'tp'=16] {'core'}, dimensions={0} | all-to-all | bytes 524288 | tf_op jit(solution)/shard_map/all_to_all | solution.py:180
  19.8 0.7 fusion.1
  20.5 0.0 all-gather.2.cloned.1.call-update
  20.5 0.0 copy-start.4
  20.6 1.3 copy.14
  21.9 1.0 copy.15
  22.9 3.6 %all-to-all-start.2 = ((bf16[16,128,128]{2,1,0:T(8,128)(2,1)}), bf16[16,128,128]{2,1,0:T(8,128)(2,1)S(1)}, u32[]{:S(2)}, u32[]{:S(2)}) async-start(bf16[16,128,128]{2,1,0:T(8,128)(2,1)} %bitcast.5), calls=%async_computation.2 | async-start | bytes 1048576 | tf_op jit(solution)/shard_map/all_to_all | solution.py:186
  26.5 0.7 fusion.later_ref
  27.1 55.7 %all-gather.2.cloned.1.call-done.kv_ref = bf16[8192,128]{1,0:T(8,128)(2,1)} async-done(((bf16[512,128]{1,0:T(8,128)(2,1)}), bf16[8192,128]{1,0:T(8,128)(2,1)}) %all-gather.2.cloned.1.call-update) | async-done | bytes 2097168 | tf_op jit(solution)/shard_map/all_gather | solution.py:183
  82.9 3.9 %shard_map.110 = bf16[2,16,128,128]{3,2,1,0:T(8,128)(2,1)} custom-call(s32[1]{0:T(128)} %bitcast.z_ref, bf16[512,128]{1,0:T(8,128)(2,1)} %bitcast.23, bf16[8192,128]{1,0:T(8,128)(2,1)} %all-gather.2.cloned.1.call-done.kv_ref, bf16[256,256]{1,0:T(8,128)(2,1)} %fusion.later_ref), custom_call_target="tpu_custom_call" | custom-call | tf_op jit(solution)/shard_map/pallas_call | solution.py:197
  86.8 0.0 all-to-all-done.2.ow_ref
  86.8 16.8 %all-to-all-start.1 = ((bf16[32,128,128]{2,1,0:T(8,128)(2,1)}), bf16[32,128,128]{2,1,0:T(8,128)(2,1)S(1)}, u32[]{:S(2)}, u32[]{:S(2)}) async-start(bf16[32,128,128]{2,1,0:T(8,128)(2,1)} %bitcast.15), calls=%async_computation.1 | async-start | bytes 2097152 | tf_op jit(solution)/shard_map/all_to_all | solution.py:202
  103.6 0.8 copy.16.col_ref
  104.4 2.0 shard_map.111
  106.4 0.0 copy-done
  106.4 0.6 constant_dynamic-slice_fusion.res_ref
  107.0 13.1 %all-to-all-done.1.mixed_ref = bf16[32,128,128]{2,1,0:T(8,128)(2,1)S(1)} async-done(((bf16[32,128,128]{2,1,0:T(8,128)(2,1)}), bf16[32,128,128]{2,1,0:T(8,128)(2,1)S(1)}, u32[]{:S(2)}, u32[]{:S(2)}) %all-to-all-start.1) | async-done | bytes 1048608 | tf_op jit(solution)/shard_map/all_to_all | solution.py:202
  120.1 1.0 copy-done.1
  121.1 3.1 shard_map.112
  124.2 57.7 %all_to_all.36 = bf16[32,32,128]{2,1,0:T(8,128)(2,1)S(1)} all-to-all(bf16[32,32,128]{2,1,0:T(8,128)(2,1)} %bitcast.25), channel_id=1, replica_groups=mesh['z'=16,'core'=2,'tp'=16] {'z','core'}, dimensions={0} | all-to-all | bytes 524288 | tf_op jit(solution)/shard_map/all_to_all | solution.py:210
  181.9 0.8 broadcast_in_dim.10
  182.7 53.4 %all_to_all.37.x_ref = bf16[16,1024,128]{2,1,0:T(8,128)(2,1)} all-to-all(bf16[16,1024,128]{2,1,0:T(8,128)(2,1)S(1)} %broadcast_in_dim.10), channel_id=1, replica_groups=mesh['z'=16,'core'=2,'tp'=16] {'tp'}, dimensions={0} | all-to-all | bytes 8388608 | tf_op jit(solution)/shard_map/all_to_all | solution.py:212
  236.1 9.5 %shard_map.113 = bf16[16,1024,128]{2,1,0:T(8,128)(2,1)} custom-call(bf16[16,1024,128]{2,1,0:T(8,128)(2,1)} %all_to_all.37.x_ref, f32[16,128]{1,0:T(8,128)} %bitcast.26, bf16[2048,256]{1,0:T(8,128)(2,1)} %bitcast.17, bf16[2048,256]{1,0:T(8,128)(2,1)} %bitcast.18, bf16[256,2048]{1,0:T(8,128)(2,1)} %bitcast.19), custom_call_target="tpu_custom_call" | custom-call | tf_op jit(solution)/shard_map/pallas_call | solution.py:216
  245.6 54.3 %all_to_all.38.x_ref = bf16[16,1024,128]{2,1,0:T(8,128)(2,1)} all-to-all(bf16[16,1024,128]{2,1,0:T(8,128)(2,1)} %shard_map.113), channel_id=1, replica_groups=mesh['z'=16,'core'=2,'tp'=16] {'tp'}, dimensions={0} | all-to-all | bytes 8388608 | tf_op jit(solution)/shard_map/all_to_all | solution.py:229
  300.0 4.1 %shard_map.114 = bf16[1024,128]{1,0:T(8,128)(2,1)} custom-call(bf16[16,1024,128]{2,1,0:T(8,128)(2,1)} %all_to_all.38.x_ref), custom_call_target="tpu_custom_call" | custom-call | tf_op jit(solution)/shard_map/pallas_call | solution.py:230
  304.0 7.1 %all-to-all-start.6 = ((bf16[32,32,128]{2,1,0:T(8,128)(2,1)}), bf16[32,32,128]{2,1,0:T(8,128)(2,1)S(1)}, u32[]{:S(2)}, u32[]{:S(2)}) async-start(bf16[32,32,128]{2,1,0:T(8,128)(2,1)} %bitcast.20), calls=%async_computation.6 | async-start | bytes 524288 | tf_op jit(solution)/shard_map/all_to_all | solution.py:237
  311.2 0.8 copy.17.score_ref
  312.0 21.5 %all-to-all-done.6 = bf16[32,32,128]{2,1,0:T(8,128)(2,1)S(1)} async-done(((bf16[32,32,128]{2,1,0:T(8,128)(2,1)}), bf16[32,32,128]{2,1,0:T(8,128)(2,1)S(1)}, u32[]{:S(2)}, u32[]{:S(2)}) %all-to-all-start.6) | async-done | bytes 262176 | tf_op jit(solution)/shard_map/all_to_all | solution.py:237
  333.4 0.7 copy-done.3
  334.1 2.2 shard_map.115
  (8 shorter events, 0.0 us)
Async XLA Ops:
  6.5 99.9 %copy-start = (bf16[256,2048]{1,0:T(8,128)(2,1)S(1)}, bf16[256,2048]{1,0:T(8,128)(2,1)}, u32[]{:S(2)}) copy-start(bf16[256,2048]{1,0:T(8,128)(2,1)} %param.11) | copy-start | bytes 3145732
  6.5 76.3 %all-gather.2.cloned.1.call-start = ((), (), s32[]{:S(2)}) async-start(), calls=%async_computation.7 | async-start | bytes 2228224 | tf_op jit(solution)/shard_map/all_gather | solution.py:183
  20.5 83.0 %copy-start.4 = (s32[256,2]{0,1:T(2,128)S(1)}, s32[256,2]{0,1:T(2,128)}, u32[]{:S(2)}) copy-start(s32[256,2]{0,1:T(2,128)} %param.17) | copy-start | bytes 6148
  22.9 63.9 %all-to-all-start.2 = ((bf16[16,128,128]{2,1,0:T(8,128)(2,1)}), bf16[16,128,128]{2,1,0:T(8,128)(2,1)S(1)}, u32[]{:S(2)}, u32[]{:S(2)}) async-start(bf16[16,128,128]{2,1,0:T(8,128)(2,1)} %bitcast.5), calls=%async_computation.2 | async-start | bytes 1048576 | tf_op jit(solution)/shard_map/all_to_all | solution.py:186
  86.8 33.4 %copy-start.2 = (bf16[16,128,128]{2,1,0:T(8,128)(2,1)}, bf16[16,128,128]{2,1,0:T(8,128)(2,1)S(1)}, u32[]{:S(2)}) copy-start(bf16[16,128,128]{2,1,0:T(8,128)(2,1)S(1)} %all-to-all-done.2.ow_ref) | copy-start | bytes 1572868
  86.8 33.3 %all-to-all-start.1 = ((bf16[32,128,128]{2,1,0:T(8,128)(2,1)}), bf16[32,128,128]{2,1,0:T(8,128)(2,1)S(1)}, u32[]{:S(2)}, u32[]{:S(2)}) async-start(bf16[32,128,128]{2,1,0:T(8,128)(2,1)} %bitcast.15), calls=%async_computation.1 | async-start | bytes 2097152 | tf_op jit(solution)/shard_map/all_to_all | solution.py:202
  120.1 1.0 copy-start.1
  300.0 11.2 %copy-start.5 = (f32[256,2]{0,1:T(2,128)S(1)}, f32[256,2]{0,1:T(2,128)}, u32[]{:S(2)}) copy-start(f32[256,2]{0,1:T(2,128)} %param.18) | copy-start | bytes 6148
  304.0 29.4 %all-to-all-start.6 = ((bf16[32,32,128]{2,1,0:T(8,128)(2,1)}), bf16[32,32,128]{2,1,0:T(8,128)(2,1)S(1)}, u32[]{:S(2)}, u32[]{:S(2)}) async-start(bf16[32,32,128]{2,1,0:T(8,128)(2,1)} %bitcast.20), calls=%async_computation.6 | async-start | bytes 524288 | tf_op jit(solution)/shard_map/all_to_all | solution.py:237
  333.4 0.7 copy-start.3
Sparse Core Ops, SparseCore 0:
  20.7 62.1 all-gather.1
